TPU v7x, 32 devices: a whole 2x2x4 slice. The times are simulated.
32 devices in a mesh: sp: 4 (over z), tp: 8 (over y, x, core).
Axes of the slice: x: 2, y: 2, z: 4, core: 2. Of those that a mesh axis runs over, the one named last changes fastest.
Arguments:
- tokens: bfloat16 [1536, 2048], P('sp', 'tp'), may hold values from -6 to 6
- norm_gain: bfloat16 [2048], replicated, may hold values from 0.099609375 to 1.8984375
- lin_query: bfloat16 [2048, 1024], P(None, 'tp'), may hold values from -0.125 to 0.125
- lin_key: bfloat16 [2048, 1024], P(None, 'tp'), may hold values from -0.125 to 0.125
- lin_value: bfloat16 [2048, 1024], P(None, 'tp'), may hold values from -0.125 to 0.125
- lin_gate: bfloat16 [2048, 1024], P(None, 'tp'), may hold values from -0.125 to 0.125
- gate_down: bfloat16 [2048, 32], replicated, may hold values from -0.125 to 0.125
- gate_up_weight: bfloat16 [32, 1024], replicated, may hold values from -1 to 1
- decay_offset_bias: float32 [1536, 1024], P('sp', 'tp'), may hold values from -16 to 11
- lin_norm_gain: float32 [128], replicated, may hold values from 0.1 to 1.9
- stick_query: bfloat16 [2048, 1024], P(None, 'tp'), may hold values from -0.25 to 0.25
- stick_key: bfloat16 [2048, 1024], P(None, 'tp'), may hold values from -0.25 to 0.25
- stick_value: bfloat16 [2048, 1024], P(None, 'tp'), may hold values from -0.125 to 0.125
- key_bias: bfloat16 [8, 1536], P('tp', 'sp'), may hold values from -20 to -2
- out_linear: bfloat16 [1024, 2048], replicated, may hold values from -0.125 to 0.125
- out_stick: bfloat16 [1024, 2048], replicated, may hold values from -0.125 to 0.125
Outputs:
- mixed: bfloat16 [1536, 2048], P(('sp', 'tp'))
All inputs are finite; a program needn't handle non-finite values.
Results may differ from a plain program's by a relative error of at most 0.012.
Values may be sent and summed in bfloat16 or wider, within the bound.
A program may use at most 64 MiB of HBM per device.

v0:
```python
import functools
import jax
import jax.numpy as jnp
from jax import lax
from jax.experimental import pallas as pl
from jax.experimental.pallas import tpu as pltpu
from jax.sharding import PartitionSpec as P

norm_eps = 1e-06
gate_softness = 16.0
CHUNK = 128
F32 = jnp.float32
BF16 = jnp.bfloat16
NT = (((1,), (1,)), ((), ()))
TN = (((0,), (0,)), ((), ()))


def fdot(a, b):
    return jnp.dot(a, b, preferred_element_type=F32)


def gdot(a, b, dims):
    return lax.dot_general(a, b, dims, preferred_element_type=F32)


def kernel(
    n_sp,
    n_tp,
    tokens,
    gain,
    lq_w,
    lk_w,
    lv_w,
    lg_w,
    sq_w,
    sk_w,
    sv_w,
    gd_w,
    gu_w,
    dbias,
    head_gain,
    kbias,
    ol_w,
    os_w,
    out,
    w_s,
    gd_s,
    gu_s,
    db_s,
    wol,
    wos,
    tok,
    acc,
    acc_low,
    squares,
    lin_b,
    dlog,
    qx,
    kv,
    bias_s,
    tri,
    o_acc,
    cons,
    far_o,
    far_c,
    far_out,
    ret,
    fin,
    local,
    qstart,
    st_buf,
    td_buf,
    lin_o,
    stk_o,
    lin_r,
    stk_r,
    wsem,
    tok_send,
    tok_recv,
    q_send,
    q_recv,
    ret_send,
    ret_recv,
    bias_send,
    bias_recv,
    kv_send,
    kv_recv,
    st_send,
    st_recv,
    td_send,
    td_recv,
    al_send,
    al_recv,
    as_send,
    as_recv,
):
    me = lax.axis_index("tp")
    here = lax.axis_index("sp")
    T, F = tokens.shape
    H = T // 2
    DK = lq_w.shape[1]
    D = lq_w.shape[0]
    rows_out = T // n_tp
    scale = DK ** (-0.5)
    balanced = n_sp == 4
    reach = 2 if balanced else n_sp

    copies = []
    for i, w in enumerate((sk_w, sv_w, sq_w, lq_w, lk_w, lv_w, lg_w)):
        copies.append(pltpu.make_async_copy(w, w_s.at[:, pl.ds(i * DK, DK)], wsem.at[i]))
    copies.append(pltpu.make_async_copy(gd_w, gd_s, wsem.at[7]))
    col = pl.multiple_of(me * DK, DK)
    copies.append(pltpu.make_async_copy(gu_w.at[:, pl.ds(col, DK)], gu_s, wsem.at[8]))
    copies.append(pltpu.make_async_copy(dbias, db_s, wsem.at[9]))
    copies.append(pltpu.make_async_copy(ol_w, wol, wsem.at[10]))
    copies.append(pltpu.make_async_copy(os_w, wos, wsem.at[11]))
    for c in copies:
        c.start()

    barrier = pltpu.get_barrier_semaphore()
    for d in range(1, n_tp):
        pl.semaphore_signal(
            barrier, inc=1, device_id={"tp": (me + d) % n_tp}, device_id_type=pl.DeviceIdType.MESH
        )
    for d in range(1, n_sp):
        pl.semaphore_signal(
            barrier, inc=1, device_id={"sp": (here + d) % n_sp}, device_id_type=pl.DeviceIdType.MESH
        )
    pl.semaphore_wait(barrier, n_tp + n_sp - 2)

    def remote(src, dst, send, recv, where):
        return pltpu.make_async_remote_copy(
            src_ref=src,
            dst_ref=dst,
            send_sem=send,
            recv_sem=recv,
            device_id=where,
            device_id_type=pl.DeviceIdType.MESH,
        )

    core = me % 2
    chip = me // 2
    side = 1 - 2 * core
    partner = me + side
    x_chip = chip + 1 - 2 * (chip % 2)
    y_step = 2 * (1 - 2 * (chip // 2))
    y_chip = chip + y_step
    d_chip = x_chip + y_step
    x_dev, y_dev, d_dev = 2 * x_chip + core, 2 * y_chip + core, 2 * d_chip + core

    sent = []

    def piece(ref, h):
        return ref.at[pl.ds(h * H, H)]

    def send_tok(src, h, target, own=False):
        dst = tok.at[src, pl.ds(h * H, H)]
        c = remote(
            piece(tokens, h) if own else dst,
            dst,
            tok_send.at[len(sent)],
            tok_recv.at[src, h],
            {"tp": target},
        )
        c.start()
        sent.append(c)

    def wait_tok(src, h):
        dst = tok.at[src, pl.ds(h * H, H)]
        remote(dst, dst, tok_send.at[0], tok_recv.at[src, h], {"tp": partner}).wait_recv()

    send_tok(me, 0, x_dev, True)
    send_tok(me, 1, y_dev, True)
    send_tok(me, 1, x_dev, True)
    send_tok(me, 0, y_dev, True)
    send_tok(me, 0, partner, True)
    send_tok(me, 1, partner, True)

    bias_s[here] = jnp.broadcast_to(kbias[...].astype(F32), bias_s.shape[1:])

    def later(d, make):
        @pl.when(here + d < n_sp)
        def _():
            make(d)

    def bias_copy(d):
        return remote(
            bias_s.at[here], bias_s.at[here], bias_send.at[d], bias_recv.at[here], {"sp": here + d}
        )

    for d in range(1, reach):
        later(d, lambda d: bias_copy(d).start())

    rr = lax.broadcasted_iota(jnp.int32, (T, T), 0)
    cc = lax.broadcasted_iota(jnp.int32, (T, T), 1)
    tri[...] = jnp.where(rr > cc, 1.0, 0.0).astype(BF16)

    def project(src, ref, first=False):
        at = pl.ds(pl.multiple_of(src * F, F), F)
        raw = ref[...].astype(F32)
        sq = raw * raw
        part = sq[:, :128]
        for i in range(1, F // 128):
            part = part + sq[:, i * 128 : (i + 1) * 128]
        scaled = (raw * gain[at].astype(F32)[None, :]).astype(BF16)
        main = fdot(scaled, w_s[at, :])
        low = gdot(scaled, gd_s[:, at], NT)
        if first:
            squares[...] = part
            acc[...] = main
            acc_low[...] = low
        else:
            squares[...] += part
            acc[...] += main
            acc_low[...] += low

    for i in range(8):
        copies[i].wait()
    project(me, tokens, True)
    wait_tok(partner, 0)
    wait_tok(partner, 1)
    project(partner, tok.at[partner])
    wait_tok(x_dev, 0)
    send_tok(x_dev, 0, y_dev)
    send_tok(x_dev, 0, partner)
    wait_tok(y_dev, 1)
    send_tok(y_dev, 1, x_dev)
    send_tok(y_dev, 1, partner)
    wait_tok(x_dev, 1)
    send_tok(x_dev, 1, partner)
    wait_tok(y_dev, 0)
    send_tok(y_dev, 0, partner)
    project(x_dev, tok.at[x_dev])
    project(y_dev, tok.at[y_dev])
    for p in (x_dev + side, y_dev + side):
        wait_tok(p, 0)
        wait_tok(p, 1)
        project(p, tok.at[p])
    wait_tok(d_dev, 0)
    send_tok(d_dev, 0, partner)
    wait_tok(d_dev, 1)
    send_tok(d_dev, 1, partner)
    project(d_dev, tok.at[d_dev])
    wait_tok(d_dev + side, 0)
    wait_tok(d_dev + side, 1)
    project(d_dev + side, tok.at[d_dev + side])

    inv = lax.rsqrt(jnp.sum(squares[...], axis=1, keepdims=True) / D + norm_eps)

    def proj(i):
        return (acc[:, i * DK : (i + 1) * DK] * inv).astype(BF16)

    kv[here, 0] = proj(0)
    kv[here, 1] = proj(1)

    C = CHUNK

    def kv_copy(j, s):
        return remote(kv.at[j], kv.at[j], kv_send.at[s], kv_recv.at[j], {"sp": here + 1})

    split = 0
    parts = ((split, T), (0, split)) if split else ((0, T),)

    def kv_part(j, i):
        lo, hi = parts[i]
        view = kv.at[j, :, pl.ds(lo, hi - lo)]
        return remote(view, view, kv_send.at[i], kv_recv.at[i], {"sp": here + 1})

    @pl.when(here + 1 < n_sp)
    def _():
        if balanced:
            for i in range(len(parts)):
                kv_part(here, i).start()
        else:
            kv_copy(here, 0).start()

    qx[0] = proj(2)

    def q_copy(slot):
        return remote(qx.at[0], qx.at[slot], q_send.at[slot], q_recv.at[slot], {"sp": 2 - slot})

    def ret_copy(i, r, target):
        at = pl.ds(r * C, C)
        return remote(
            far_out.at[i, at], ret.at[at], ret_send.at[i, r], ret_recv.at[r], {"sp": target}
        )

    if balanced:

        @pl.when(here == 3)
        def _():
            q_copy(1).start()

        @pl.when(here == 2)
        def _():
            q_copy(2).start()

    for i in range(4):
        lin_b[i] = proj(3 + i)
    for i in range(8, 10):
        copies[i].wait()
    low = (acc_low[...] * inv).astype(BF16)
    pre = fdot(low, gu_s[...]) + db_s[...]
    dlog[...] = (
        jnp.minimum(pre, 0.0) - jnp.log(1.0 + jnp.exp(-jnp.abs(pre)))
    ) / gate_softness

    row = lax.broadcasted_iota(jnp.int32, (C, DK), 0)
    rc = lax.broadcasted_iota(jnp.int32, (C, C), 0)
    ccol = lax.broadcasted_iota(jnp.int32, (C, C), 1)
    tri_c = jnp.where(rc >= ccol, 1.0, 0.0).astype(F32)

    def chunk(n, carry):
        state, offset = carry
        at = pl.ds(pl.multiple_of(n * C, C), C)
        lam = dlog[at, :]
        c = jnp.dot(tri_c, lam, preferred_element_type=F32, precision=lax.Precision.HIGHEST)
        q = lin_b[0, at, :].astype(F32) * scale
        k = lin_b[1, at, :].astype(F32)
        v = lin_b[2, at, :]
        v32 = v.astype(F32)
        scores = jnp.zeros((C, C), F32)
        m = C // 2
        while m >= 8:
            grouped = c.reshape(C // (2 * m), 2 * m, DK)
            middle = jnp.broadcast_to(grouped[:, m - 1 : m, :], grouped.shape).reshape(C, DK)
            upper = row % (2 * m) >= m
            a = jnp.where(upper, q, k) * jnp.exp(jnp.where(upper, c - middle, middle - c))
            ab = a.astype(BF16)
            pair = gdot(ab, ab, NT)
            keep = (
                (rc // (2 * m) == ccol // (2 * m))
                & (rc % (2 * m) >= m)
                & (ccol % (2 * m) < m)
            )
            scores = jnp.where(keep, pair, scores)
            m //= 2
        total = fdot(scores.astype(BF16), v)
        for delta in range(8):
            if delta == 0:
                p = jnp.sum(q * k, axis=1, keepdims=True)
                total = total + p * v32
                continue
            kd = pltpu.roll(k, delta, 0)
            cd = pltpu.roll(c, delta, 0)
            vd = pltpu.roll(v32, delta, 0)
            p = jnp.sum(q * kd * jnp.exp(jnp.minimum(c - cd, 0.0)), axis=1, keepdims=True)
            total = total + jnp.where(row % 8 >= delta, p * vd, 0.0)
        total = total + gdot((q * jnp.exp(c)).astype(BF16), state.astype(BF16), NT)
        local[at, :] = total
        qstart[at, :] = (q * jnp.exp(offset + c)).astype(BF16)
        last = c[C - 1 : C, :]
        kk = (k * jnp.exp(last - c)).astype(BF16)
        state = state * jnp.exp(last) + gdot(v, kk, TN)
        return state, offset + last

    state, offset = lax.fori_loop(
        0, T // C, chunk, (jnp.zeros((DK, DK), F32), jnp.zeros((1, DK), F32))
    )
    st_buf[here] = state.astype(BF16)
    td_buf[here] = jnp.broadcast_to(offset, td_buf.shape[1:])

    def st_copy(d):
        return remote(
            st_buf.at[here], st_buf.at[here], st_send.at[d], st_recv.at[here], {"sp": here + d}
        )

    def td_copy(d):
        return remote(
            td_buf.at[here], td_buf.at[here], td_send.at[d], td_recv.at[here], {"sp": here + d}
        )

    for d in range(n_sp - 1, 0, -1):
        later(d, lambda d: st_copy(d).start())
        later(d, lambda d: td_copy(d).start())

    def stick(slot, j, mode, o_ref, c_ref, keys=(0, T), finish=None):
        own = mode == "own"
        lo = keys[0]
        for r in range(T // C):
            at = pl.ds(r * C, C)
            n = (r + 1) * C if own else keys[1] - lo
            bias = bias_s[j, 0:1, pl.ds(lo, n)]
            z = gdot(qx[slot, at, :], kv[j, 0, pl.ds(lo, n), :], NT) * scale + bias
            soft = jnp.log(1.0 + jnp.exp(-jnp.abs(z)))
            rise = jnp.minimum(z, 0.0) - soft
            fall = jnp.minimum(-z, 0.0) - soft
            if own:
                tr = lax.broadcasted_iota(jnp.int32, (C, n), 0) + r * C
                visible = lax.broadcasted_iota(jnp.int32, (C, n), 1) < tr
                fall = jnp.where(visible, fall, 0.0)
            high = fall.astype(BF16)
            rest = (fall - high.astype(F32)).astype(BF16)
            later_keys = tri[pl.ds(0, n), pl.ds(0, n)]
            behind = fdot(high, later_keys) + fdot(rest, later_keys)
            power = rise + behind
            if mode == "add":
                power = power + c_ref[at, 0:1]
            share = jnp.exp(power)
            if own:
                share = jnp.where(visible, share, 0.0)
            value = fdot(share.astype(BF16), kv[j, 1, pl.ds(lo, n), :])
            spent = jnp.broadcast_to(behind[:, 0:1] + fall[:, 0:1], (C, DK))
            if mode == "add":
                value = value + o_ref[at, :]
                spent = spent + c_ref[at, :]
            if finish is None:
                o_ref[at, :] = value
                c_ref[at, :] = spent
            else:
                finish(r, value)

    stick(0, here, "own", o_acc, cons)

    def await_kv(j, s):
        remote(kv.at[j], kv.at[j], kv_send.at[s], kv_recv.at[j], {"sp": here}).wait_recv()

    def await_bias(j):
        remote(
            bias_s.at[j], bias_s.at[j], bias_send.at[0], bias_recv.at[j], {"sp": here}
        ).wait_recv()

    def take(s):
        j = here - s
        await_kv(j, s)

        @pl.when(here + 1 < n_sp)
        def _():
            kv_copy(j, s).start()

        await_bias(j)
        stick(0, j, "add", o_acc, cons)

    def give(i, target):
        def finish(r, value):
            far_out[i, pl.ds(r * C, C), :] = value.astype(BF16)
            ret_copy(i, r, target).start()

        return finish

    if balanced:
        last = len(parts) - 1

        @pl.when(here == 1)
        def _():
            q_copy(1).wait_recv()
            stick(1, 1, "start", far_o, far_c)
            await_bias(0)
            for i in range(len(parts)):
                kv_part(0, i).wait_recv()
                stick(1, 0, "add", far_o, far_c, parts[i], give(0, 3) if i == last else None)

        @pl.when(here == 0)
        def _():
            q_copy(2).wait_recv()
            stick(2, 0, "start", far_o, far_c, finish=give(1, 2))

        @pl.when(here >= 2)
        def _():
            await_bias(here - 1)
            for i in range(len(parts)):
                kv_part(here - 1, i).wait_recv()
            stick(0, here - 1, "add", o_acc, cons)

    else:

        @pl.when(here >= 1)
        def _():
            take(1)

    def gather_state(j, incoming):
        remote(st_buf.at[j], st_buf.at[j], st_send.at[0], st_recv.at[j], {"sp": here}).wait_recv()
        remote(td_buf.at[j], td_buf.at[j], td_send.at[0], td_recv.at[j], {"sp": here}).wait_recv()
        return incoming * jnp.exp(td_buf[j][0:1, :]) + st_buf[j].astype(F32)

    incoming = lax.fori_loop(0, here, gather_state, jnp.zeros((DK, DK), F32))
    combined = local[...] + gdot(qstart[...], incoming.astype(BF16), NT)
    normed = (
        combined
        * lax.rsqrt(jnp.mean(combined * combined, axis=1, keepdims=True) + norm_eps)
        * head_gain[...]
    )
    gate = lin_b[3].astype(F32)
    lin_o[...] = (normed * (gate / (1.0 + jnp.exp(-gate)))).astype(BF16)

    def exchange(source, landing, send, recv):
        done = []
        for d in range(1, n_tp):
            p = (me + d) % n_tp
            c = remote(
                source.at[pl.ds(pl.multiple_of(p * rows_out, rows_out), rows_out)],
                landing.at[me],
                send.at[d],
                recv.at[me],
                {"tp": p},
            )
            c.start()
            done.append(c)
        own = pl.ds(pl.multiple_of(me * rows_out, rows_out), rows_out)
        landing[me] = source[own, :]
        return done

    def arrive(landing, recv):
        for d in range(1, n_tp):
            p = (me + d) % n_tp
            remote(landing.at[p], landing.at[p], recv.at[p], recv.at[p], {"tp": p}).wait_recv()

    lin_sent = exchange(lin_o, lin_r, al_send, al_recv)

    if balanced:

        @pl.when(here == 1)
        def _():
            stick(0, 0, "add", o_acc, cons)

        @pl.when(here >= 2)
        def _():
            for r in range(T // C):
                ret_copy(0, r, here).wait_recv()
            o_acc[...] += jnp.exp(cons[...]) * ret[...].astype(F32)

    else:

        def more(s, carry):
            take(s)
            return carry

        lax.fori_loop(2, here + 1, more, 0)

    stk_o[...] = o_acc[...].astype(BF16)
    stk_sent = exchange(stk_o, stk_r, as_send, as_recv)
    copies[10].wait()
    copies[11].wait()
    arrive(lin_r, al_recv)

    def gathered(landing):
        return jnp.concatenate([landing[p] for p in range(n_tp)], axis=1)

    fin[...] = fdot(gathered(lin_r), wol[...])
    arrive(stk_r, as_recv)
    out[...] = (fin[...] + fdot(gathered(stk_r), wos[...])).astype(BF16)

    for c in sent + lin_sent + stk_sent:
        c.wait_send()
    for d in range(1, reach):
        later(d, lambda d: bias_copy(d).wait_send())
    for d in range(1, n_sp):
        later(d, lambda d: st_copy(d).wait_send())
        later(d, lambda d: td_copy(d).wait_send())

    @pl.when(here + 1 < n_sp)
    def _():
        if balanced:
            for i in range(len(parts)):
                kv_part(here, i).wait_send()
        else:

            def drain(s, carry):
                kv_copy(here - s, s).wait_send()
                return carry

            lax.fori_loop(0, here + 1, drain, 0)

    if balanced:

        @pl.when(here == 3)
        def _():
            q_copy(1).wait_send()

        @pl.when(here == 2)
        def _():
            q_copy(2).wait_send()

        @pl.when(here == 1)
        def _():
            for r in range(T // C):
                ret_copy(0, r, 3).wait_send()

        @pl.when(here == 0)
        def _():
            for r in range(T // C):
                ret_copy(1, r, 2).wait_send()


def per_device(n_sp, n_tp, *args):
    (
        tokens,
        norm_gain,
        lin_query,
        lin_key,
        lin_value,
        lin_gate,
        gate_down,
        gate_up_weight,
        decay_offset_bias,
        lin_norm_gain,
        stick_query,
        stick_key,
        stick_value,
        key_bias,
        out_linear,
        out_stick,
    ) = args
    T, F = tokens.shape
    D, DK = lin_query.shape
    rank = gate_down.shape[1]
    rows_out = T // n_tp
    width = out_linear.shape[1]
    vm = pl.BlockSpec(memory_space=pltpu.VMEM)
    anywhere = pl.BlockSpec(memory_space=pl.ANY)
    dma = pltpu.SemaphoreType.DMA
    return pl.pallas_call(
        functools.partial(kernel, n_sp, n_tp),
        out_shape=jax.ShapeDtypeStruct((rows_out, width), BF16),
        in_specs=[vm, vm] + [anywhere] * 10 + [vm, vm, anywhere, anywhere],
        out_specs=vm,
        scratch_shapes=[
            pltpu.VMEM((D, 7 * DK), BF16),
            pltpu.VMEM((rank, D), BF16),
            pltpu.VMEM((rank, DK), BF16),
            pltpu.VMEM((T, DK), F32),
            pltpu.VMEM(out_linear.shape, BF16),
            pltpu.VMEM(out_stick.shape, BF16),
            pltpu.VMEM((n_tp, T, F), BF16),
            pltpu.VMEM((T, 7 * DK), F32),
            pltpu.VMEM((T, rank), F32),
            pltpu.VMEM((T, 128), F32),
            pltpu.VMEM((4, T, DK), BF16),
            pltpu.VMEM((T, DK), F32),
            pltpu.VMEM((3, T, DK), BF16),
            pltpu.VMEM((n_sp, 2, T, DK), BF16),
            pltpu.VMEM((n_sp, 8, T), F32),
            pltpu.VMEM((T, T), BF16),
            pltpu.VMEM((T, DK), F32),
            pltpu.VMEM((T, DK), F32),
            pltpu.VMEM((T, DK), F32),
            pltpu.VMEM((T, DK), F32),
            pltpu.VMEM((2, T, DK), BF16),
            pltpu.VMEM((T, DK), BF16),
            pltpu.VMEM((rows_out, width), F32),
            pltpu.VMEM((T, DK), F32),
            pltpu.VMEM((T, DK), BF16),
            pltpu.VMEM((n_sp, DK, DK), BF16),
            pltpu.VMEM((n_sp, 8, DK), F32),
            pltpu.VMEM((T, DK), BF16),
            pltpu.VMEM((T, DK), BF16),
            pltpu.VMEM((n_tp, rows_out, DK), BF16),
            pltpu.VMEM((n_tp, rows_out, DK), BF16),
            dma((12,)),
            dma((16,)),
            dma((n_tp, 2)),
            dma((3,)),
            dma((3,)),
            dma((2, T // CHUNK)),
            dma((T // CHUNK,)),
            dma((n_sp,)),
            dma((n_sp,)),
            dma((n_sp,)),
            dma((n_sp,)),
            dma((n_sp,)),
            dma((n_sp,)),
            dma((n_sp,)),
            dma((n_sp,)),
            dma((n_tp,)),
            dma((n_tp,)),
            dma((n_tp,)),
            dma((n_tp,)),
        ],
        compiler_params=pltpu.CompilerParams(collective_id=0, has_side_effects=True),
    )(
        tokens,
        norm_gain,
        lin_query,
        lin_key,
        lin_value,
        lin_gate,
        stick_query,
        stick_key,
        stick_value,
        gate_down.T,
        gate_up_weight,
        decay_offset_bias,
        lin_norm_gain.reshape(1, DK),
        key_bias,
        out_linear,
        out_stick,
    )


def solution(mesh):
    placed = (
        P("sp", "tp"),
        P(),
        P(None, "tp"),
        P(None, "tp"),
        P(None, "tp"),
        P(None, "tp"),
        P(),
        P(),
        P("sp", "tp"),
        P(),
        P(None, "tp"),
        P(None, "tp"),
        P(None, "tp"),
        P("tp", "sp"),
        P(),
        P(),
    )
    return jax.shard_map(
        functools.partial(per_device, mesh.shape["sp"], mesh.shape["tp"]),
        mesh=mesh,
        in_specs=placed,
        out_specs=P(("sp", "tp"), None),
        check_vma=False,
    )
```

profile of v0, /device:TPU:25, one launch (start us, length us, event | category | flops | bytes accessed | tf_op | source)
XLA Modules:
  0.0 35.2 jit_solution(12526626862131810811)
XLA Ops:
  0.0 33.6 %shard_map.154 = bf16[48,2048]{1,0:T(8,128)(2,1)} custom-call(bf16[384,256]{1,0:T(8,128)(2,1)} %tokens.1, bf16[2048]{0:T(1024)(128)(2,1)} %gain.1, bf16[2048,128]{1,0:T(8,128)(2,1)} %lq_w.1, bf16[2048,128]{1,0:T(8,128)(2,1)} %lk_w.1, bf16[2048,128]{1,0:T(8,128)(2,1)} %lv_w.1, bf16[2048,128]{1,0:T(8,128)(2,1)} %lg_w.1, bf16[2048,128]{1,0:T(8,128)(2,1)} %sq_w.1, ...), custom_call_target="tpu_custom_call" | custom-call | tf_op jit(solution)/shard_map/pallas_call | solution.py:612
  33.6 1.6 %copy.18 = bf16[48,2048]{1,0:T(8,128)(2,1)} copy(bf16[48,2048]{1,0:T(8,128)(2,1)} %shard_map.154) | data formatting | bytes 393216
where the time goes:
time: 35.3 us; the launch traced here: 35.2 us
  Pallas kernels  33.6 us (95%)
  local copies, waits for them, and re-layouts  1.62 us (5%)
    pallas_call x1, Pallas kernels, per_device(): pl.pallas_call(functools.partial(kernel, n_sp, n_tp), out_shape=jax.Shape...  33.6 us
    unnamed x1, local copies, waits for them, and re-layouts  1.62 us

commit v1 on v0

--- a/solution.py
+++ b/solution.py
@@ -611,7 +611,7 @@
     dma = pltpu.SemaphoreType.DMA
     return pl.pallas_call(
         functools.partial(kernel, n_sp, n_tp),
-        out_shape=jax.ShapeDtypeStruct((rows_out, width), BF16),
+        out_shape=pltpu.VMEM((rows_out, width), BF16),
         in_specs=[vm, vm] + [anywhere] * 10 + [vm, vm, anywhere, anywhere],
         out_specs=vm,
         scratch_shapes=[

time: 35.3 us -> 33.7 us (0.955)
  local copies, waits for them, and re-layouts: 1.62 us -> 0.68 us
  Pallas kernels: 33.6 us -> 32.9 us
    unnamed x1, local copies, waits for them, and re-layouts: 1.62 us -> 0.68 us
    pallas_call x1, Pallas kernels: 33.6 us -> 32.9 us  [per_device(): pl.pallas_call(functools.partial(kernel, n_sp, n_tp), out_shape=pltpu.VME...]
where the time goes in v1:
time: 33.7 us; the launch traced here: 33.6 us
  Pallas kernels  32.9 us (98%)
  local copies, waits for them, and re-layouts  0.68 us (2%)
    pallas_call x1, Pallas kernels, per_device(): pl.pallas_call(functools.partial(kernel, n_sp, n_tp), out_shape=pltpu.VME...  32.9 us
    unnamed x1, local copies, waits for them, and re-layouts  0.68 us

profile of v1, /device:TPU:25, one launch (start us, length us, event | category | flops | bytes accessed | tf_op | source)
XLA Modules:
  0.0 33.6 jit_solution(11741444967995360882)
XLA Ops:
  0.0 32.9 %shard_map.154 = bf16[48,2048]{1,0:T(8,128)(2,1)S(1)} custom-call(bf16[384,256]{1,0:T(8,128)(2,1)} %tokens.1, bf16[2048]{0:T(1024)(128)(2,1)} %gain.1, bf16[2048,128]{1,0:T(8,128)(2,1)} %lq_w.1, bf16[2048,128]{1,0:T(8,128)(2,1)} %lk_w.1, bf16[2048,128]{1,0:T(8,128)(2,1)} %lv_w.1, bf16[2048,128]{1,0:T(8,128)(2,1)} %lg_w.1, bf16[2048,128]{1,0:T(8,128)(2,1)} %sq_w.1, ...), custom_call_target="tpu_custom_call" | custom-call | tf_op jit(solution)/shard_map/pallas_call | solution.py:612
  32.9 0.7 %copy.18 = bf16[48,2048]{1,0:T(8,128)(2,1)} copy(bf16[48,2048]{1,0:T(8,128)(2,1)S(1)} %shard_map.154) | data formatting | bytes 393216

commit v2 on v1

--- a/solution.py
+++ b/solution.py
@@ -9,6 +9,7 @@
 norm_eps = 1e-06
 gate_softness = 16.0
 CHUNK = 128
+LOG2E = 1.4426950408889634
 F32 = jnp.float32
 BF16 = jnp.bfloat16
 NT = (((1,), (1,)), ((), ()))
@@ -582,6 +583,686 @@
                 ret_copy(1, r, 2).wait_send()
 
 
+def pipelined(
+    n_sp,
+    n_tp,
+    tokens,
+    gain,
+    lq_w,
+    lk_w,
+    lv_w,
+    lg_w,
+    sq_w,
+    sk_w,
+    sv_w,
+    gd_w,
+    gu_w,
+    dbias,
+    head_gain,
+    kbias,
+    ol_w,
+    os_w,
+    out,
+    gain_s,
+    hg_s,
+    kb_s,
+    w_s,
+    gd_s,
+    gu_s,
+    db_s,
+    wol,
+    wos,
+    tok,
+    acc,
+    squares,
+    lin_b,
+    lams,
+    cums,
+    qe,
+    qstart,
+    snap,
+    state_s,
+    offset_s,
+    qx,
+    kv,
+    bias_s,
+    tri,
+    o_acc,
+    cons,
+    near,
+    decay,
+    far,
+    local,
+    st_buf,
+    lin_o,
+    lin_r,
+    near_r,
+    decay_r,
+    far_r,
+    fin,
+    wsem,
+    tok_send,
+    tok_recv,
+    q_send,
+    q_recv,
+    bias_send,
+    bias_recv,
+    kv_send,
+    kv_recv,
+    st_send,
+    st_recv,
+    al_send,
+    al_recv,
+    an_send,
+    an_recv,
+    ad_send,
+    ad_recv,
+    af_send,
+    af_recv,
+):
+    me = lax.axis_index("tp")
+    here = lax.axis_index("sp")
+    T, F = tokens.shape
+    C = CHUNK
+    HALF = C // 2
+    NC = T // C
+    DK = lq_w.shape[1]
+    D = lq_w.shape[0]
+    rank = gd_w.shape[0]
+    rows_out = T // n_tp
+    scale = DK ** (-0.5)
+
+    barrier = pltpu.get_barrier_semaphore()
+    for d in range(1, n_tp):
+        pl.semaphore_signal(
+            barrier, inc=1, device_id={"tp": (me + d) % n_tp}, device_id_type=pl.DeviceIdType.MESH
+        )
+    for d in range(1, n_sp):
+        pl.semaphore_signal(
+            barrier, inc=1, device_id={"sp": (here + d) % n_sp}, device_id_type=pl.DeviceIdType.MESH
+        )
+
+    copies = [pltpu.make_async_copy(tokens, tok.at[me], wsem.at[12])]
+    copies.append(pltpu.make_async_copy(gain, gain_s, wsem.at[13]))
+    copies.append(pltpu.make_async_copy(kbias, kb_s, wsem.at[14]))
+    for i, w in enumerate((sk_w, sv_w, sq_w, lq_w, lk_w, lv_w, lg_w)):
+        copies.append(pltpu.make_async_copy(w, w_s.at[:, pl.ds(i * DK, DK)], wsem.at[i]))
+    copies.append(pltpu.make_async_copy(gd_w, gd_s, wsem.at[7]))
+    col = pl.multiple_of(me * DK, DK)
+    late = [pltpu.make_async_copy(gu_w.at[:, pl.ds(col, DK)], gu_s, wsem.at[8])]
+    late.append(pltpu.make_async_copy(dbias, db_s, wsem.at[9]))
+    late.append(pltpu.make_async_copy(head_gain, hg_s, wsem.at[15]))
+    wide = [pltpu.make_async_copy(ol_w, wol, wsem.at[10])]
+    wide.append(pltpu.make_async_copy(os_w, wos, wsem.at[11]))
+    for c in copies + late:
+        c.start()
+
+    def remote(src, dst, send, recv, where):
+        return pltpu.make_async_remote_copy(
+            src_ref=src,
+            dst_ref=dst,
+            send_sem=send,
+            recv_sem=recv,
+            device_id=where,
+            device_id_type=pl.DeviceIdType.MESH,
+        )
+
+    core = me % 2
+    chip = me // 2
+    side = 1 - 2 * core
+    partner = me + side
+    x_chip = chip + 1 - 2 * (chip % 2)
+    y_step = 2 * (1 - 2 * (chip // 2))
+    y_chip = chip + y_step
+    d_chip = x_chip + y_step
+    x_dev, y_dev, d_dev = 2 * x_chip + core, 2 * y_chip + core, 2 * d_chip + core
+
+    sent = []
+
+    def tok_at(src, i, n):
+        return tok.at[src, pl.ds(i * HALF, n * HALF)]
+
+    def send_tok(src, i, n, target):
+        at = tok_at(src, i, n)
+        c = remote(at, at, tok_send.at[len(sent)], tok_recv.at[src, i], {"tp": target})
+        c.start()
+        sent.append(c)
+
+    def wait_tok(src, i, n=1):
+        at = tok_at(src, i, n)
+        remote(at, at, tok_send.at[0], tok_recv.at[src, i], {"tp": partner}).wait_recv()
+
+    def own(i):
+        send_tok(me, i, 1, x_dev)
+        send_tok(me, i ^ 1, 1, y_dev)
+
+    copies[0].wait()
+    pl.semaphore_wait(barrier, n_tp + n_sp - 2)
+    own(0)
+    own(1)
+    for c in range(1, NC):
+        own(2 * c)
+    for c in range(NC):
+        send_tok(me, 2 * c, 2, partner)
+
+    copies[1].wait()
+    copies[2].wait()
+    bias_s[0] = jnp.broadcast_to(kb_s[...].astype(F32) * LOG2E, bias_s.shape[1:])
+
+    def later(d, make):
+        @pl.when(here + d < n_sp)
+        def _():
+            make(d)
+
+    def bias_copy():
+        return remote(
+            bias_s.at[0], bias_s.at[1], bias_send.at[0], bias_recv.at[0], {"sp": here + 1}
+        )
+
+    later(1, lambda d: bias_copy().start())
+
+    rr = lax.broadcasted_iota(jnp.int32, (2 * C, 2 * C), 0)
+    cc = lax.broadcasted_iota(jnp.int32, (2 * C, 2 * C), 1)
+    tri[...] = jnp.where((rr % C >= cc) | (cc >= C), 1.0, 0.0).astype(BF16)
+
+    for c in copies[3:]:
+        c.wait()
+    for c in wide:
+        c.start()
+    pick = jnp.where(
+        lax.broadcasted_iota(jnp.int32, (rank, DK), 0)
+        == lax.broadcasted_iota(jnp.int32, (rank, DK), 1),
+        1.0,
+        0.0,
+    ).astype(BF16)
+    w_s[:, pl.ds(7 * DK, DK)] = gdot(gd_s[...], pick, TN).astype(BF16)
+
+    def scaled(src, c):
+        at = pl.ds(pl.multiple_of(src * F, F), F)
+        raw = tok[src, pl.ds(c * C, C), :].astype(F32)
+        sq = raw * raw
+        part = sq[:, :128]
+        for i in range(1, F // 128):
+            part = part + sq[:, i * 128 : (i + 1) * 128]
+        return (raw * gain_s[at].astype(F32)[None, :]).astype(BF16), part, at
+
+    def group(c, srcs, first=False):
+        rows = pl.ds(c * C, C)
+        terms = [scaled(s, c) for s in srcs]
+        part = terms[0][1] + terms[1][1]
+        main = fdot(terms[0][0], w_s[terms[0][2], :]) + fdot(terms[1][0], w_s[terms[1][2], :])
+        if first:
+            squares[rows, :] = part
+            acc[rows, :] = main
+        else:
+            squares[rows, :] += part
+            acc[rows, :] += main
+
+    def kv_copy(c):
+        rows = pl.ds(c * C, C)
+        return remote(
+            kv.at[0, :, rows], kv.at[1, :, rows], kv_send.at[c], kv_recv.at[c], {"sp": here + 1}
+        )
+
+    def q_copy(c):
+        rows = pl.ds(c * C, C)
+        return remote(qx.at[0, rows], qx.at[1, rows], q_send.at[c], q_recv.at[c], {"sp": here - 2})
+
+    def finish(c, srcs):
+        rows = pl.ds(c * C, C)
+        terms = [scaled(s, c) for s in srcs]
+        square = squares[rows, :] + terms[0][1] + terms[1][1]
+        inv = lax.rsqrt(jnp.sum(square, axis=1, keepdims=True) / D + norm_eps)
+
+        def columns(h):
+            at = pl.ds(h * 4 * DK, 4 * DK)
+            total = acc[rows, at]
+            for x, _, w_at in terms:
+                total = total + fdot(x, w_s[w_at, at])
+            return (total * inv).astype(BF16)
+
+        head = columns(0)
+        kv[0, 0, rows, :] = head[:, :DK]
+        kv[0, 1, rows, :] = head[:, DK : 2 * DK]
+        qx[0, rows, :] = head[:, 2 * DK : 3 * DK]
+        later(1, lambda d: kv_copy(c).start())
+
+        @pl.when(here >= 2)
+        def _():
+            q_copy(c).start()
+
+        tail = columns(1)
+        lin_b[0, rows, :] = head[:, 3 * DK :]
+        for i in range(3):
+            lin_b[1 + i, rows, :] = tail[:, i * DK : (i + 1) * DK]
+        pre = fdot(tail[:, 3 * DK : 3 * DK + rank], gu_s[...]) + db_s[rows, :]
+        lams[rows, :] = (
+            jnp.minimum(pre, 0.0) - jnp.log(1.0 + jnp.exp(-jnp.abs(pre)))
+        ) / gate_softness
+
+    xs, ys, ds = x_dev + side, y_dev + side, d_dev + side
+
+    for c in range(NC):
+        wait_tok(partner, 2 * c, 2)
+        group(c, (me, partner), True)
+
+    def turn(c):
+        wait_tok(x_dev, 2 * c)
+        send_tok(x_dev, 2 * c, 1, y_dev)
+        wait_tok(y_dev, 2 * c + 1)
+        send_tok(y_dev, 2 * c + 1, 1, x_dev)
+        if c + 1 < NC:
+            own(2 * c + 3)
+
+    def share_chip(c):
+        wait_tok(x_dev, 2 * c + 1)
+        send_tok(x_dev, 2 * c, 2, partner)
+        wait_tok(y_dev, 2 * c)
+        send_tok(y_dev, 2 * c, 2, partner)
+
+    def share_far(c):
+        wait_tok(d_dev, 2 * c)
+        send_tok(d_dev, 2 * c, 1, partner)
+        wait_tok(d_dev, 2 * c + 1)
+        send_tok(d_dev, 2 * c + 1, 1, partner)
+
+    def side_chips(c):
+        wait_tok(xs, 2 * c, 2)
+        wait_tok(ys, 2 * c, 2)
+        group(c, (xs, ys))
+
+    def last_chip(c):
+        wait_tok(ds, 2 * c)
+        wait_tok(ds, 2 * c + 1)
+        finish(c, (d_dev, ds))
+
+    row = lax.broadcasted_iota(jnp.int32, (C, DK), 0)
+    rc = lax.broadcasted_iota(jnp.int32, (C, C), 0)
+    ccol = lax.broadcasted_iota(jnp.int32, (C, C), 1)
+
+    def advance(c):
+        rows = pl.ds(c * C, C)
+        lam = lams[rows, :]
+        high = lam.astype(BF16)
+        rest = lam - high.astype(F32)
+        mid = rest.astype(BF16)
+        low = (rest - mid.astype(F32)).astype(BF16)
+        lower = jnp.where(rc >= ccol, 1.0, 0.0).astype(BF16)
+        cum = fdot(jnp.concatenate([lower, lower], axis=1), jnp.concatenate([high, mid], axis=0))
+        cum = cum + fdot(lower, low)
+        cums[rows, :] = cum
+        q = lin_b[0, rows, :].astype(F32) * scale
+        k = lin_b[1, rows, :].astype(F32)
+        v = lin_b[2, rows, :]
+        qe[rows, :] = (q * jnp.exp(cum)).astype(BF16)
+        last = cum[C - 1 : C, :]
+        kk = (k * jnp.exp(last - cum)).astype(BF16)
+        fresh = gdot(v, kk, TN)
+        if c == 0:
+            qstart[rows, :] = (q * jnp.exp(cum)).astype(BF16)
+            state_s[...] = fresh
+            offset_s[...] = jnp.broadcast_to(last, offset_s.shape)
+        else:
+            offset = offset_s[0:1, :]
+            qstart[rows, :] = (q * jnp.exp(offset + cum)).astype(BF16)
+            snap[c] = state_s[...].astype(BF16)
+            state_s[...] = state_s[...] * jnp.exp(last) + fresh
+            offset_s[...] = jnp.broadcast_to(offset + last, offset_s.shape)
+
+    turn(0)
+    share_chip(0)
+    group(0, (x_dev, y_dev))
+    turn(1)
+    turn(2)
+    share_far(0)
+    side_chips(0)
+    share_chip(1)
+    for c in late:
+        c.wait()
+    last_chip(0)
+    group(1, (x_dev, y_dev))
+    share_far(1)
+    share_chip(2)
+    side_chips(1)
+    last_chip(1)
+    group(2, (x_dev, y_dev))
+    share_far(2)
+    advance(0)
+    side_chips(2)
+    last_chip(2)
+    advance(1)
+    advance(2)
+
+    st_buf[here, pl.ds(0, DK), :] = state_s[...].astype(BF16)
+    gone = jnp.exp(offset_s[...])
+    gone_high = gone.astype(BF16)
+    gone_low = (gone - gone_high.astype(F32)).astype(BF16)
+    st_buf[here, pl.ds(DK, 16), :] = jnp.concatenate([gone_high, gone_low], axis=0)
+
+    def st_copy(d):
+        return remote(
+            st_buf.at[here], st_buf.at[here], st_send.at[d], st_recv.at[here], {"sp": here + d}
+        )
+
+    for d in range(n_sp - 1, 0, -1):
+        later(d, lambda d: st_copy(d).start())
+
+    def within(c):
+        rows = pl.ds(c * C, C)
+        cum = cums[rows, :]
+        lam = lams[rows, :]
+        qb = lin_b[0, rows, :]
+        kb = lin_b[1, rows, :]
+        v = lin_b[2, rows, :]
+        q = qb.astype(F32) * scale
+        k = kb.astype(F32)
+        apart = rc ^ ccol
+        scores = gdot(qb, kb, NT) * scale
+        m = 1
+        while m < C:
+            upper = row % (2 * m) >= m
+            if m == 1:
+                gap = jnp.where(upper, lam, 0.0)
+            elif m == 2:
+                at = row % 4
+                before = pltpu.roll(lam, 1, 0)
+                after = pltpu.roll(lam, C - 1, 0)
+                gap = jnp.where(upper, jnp.where(at == 3, lam + before, lam), 0.0)
+                gap = jnp.where(at == 0, after, gap)
+            else:
+                grouped = cum.reshape(C // (2 * m), 2 * m, DK)
+                middle = jnp.broadcast_to(grouped[:, m - 1 : m, :], grouped.shape).reshape(C, DK)
+                gap = jnp.where(upper, cum - middle, middle - cum)
+            a = (jnp.where(upper, q, k) * jnp.exp(gap)).astype(BF16)
+            scores = jnp.where(apart >= m, gdot(a, a, NT), scores)
+            m *= 2
+        scores = jnp.where(rc >= ccol, scores, 0.0).astype(BF16)
+        total = fdot(scores, v)
+        if c:
+            total = total + gdot(qe[rows, :], snap[c], NT)
+        local[rows, :] = total
+
+    def stick(q, slot, nb, diagonal, run):
+        n = nb * C
+        z = gdot(q, kv[slot, 0, pl.ds(0, n), :], NT) * (scale * LOG2E) + bias_s[
+            slot, 0:1, pl.ds(0, n)
+        ]
+        loss = jnp.maximum(z, 0.0) + jnp.log(1.0 + jnp.exp2(-jnp.abs(z))) * LOG2E
+        shares = []
+        for b in reversed(range(nb)):
+            at = slice(b * C, (b + 1) * C)
+            piece = loss[:, at]
+            masked = diagonal and b == nb - 1
+            if masked:
+                piece = jnp.where(ccol < rc, piece, 0.0)
+            high = piece.astype(BF16)
+            rest = (piece - high.astype(F32)).astype(BF16)
+            sums = fdot(jnp.concatenate([high, rest], axis=1), tri[...])
+            power = z[:, at] - sums[:, :C]
+            if run is not None:
+                power = power - run
+            share = jnp.exp2(power)
+            if masked:
+                share = jnp.where(ccol < rc, share, 0.0)
+            shares.append(share.astype(BF16))
+            run = sums[:, C:] if run is None else run + sums[:, C:]
+        shares = jnp.concatenate(shares[::-1], axis=1) if nb > 1 else shares[0]
+        return fdot(shares, kv[slot, 1, pl.ds(0, n), :]), run
+
+    for c in range(NC):
+        within(c)
+    for r in range(NC):
+        rows = pl.ds(r * C, C)
+        o_acc[rows, :], cons[rows, :] = stick(qx[0, rows, :], 0, r + 1, True, None)
+
+    def await_kv():
+        remote(
+            bias_s.at[1], bias_s.at[1], bias_send.at[0], bias_recv.at[0], {"sp": here}
+        ).wait_recv()
+        for c in range(NC):
+            rows = pl.ds(c * C, C)
+            at = kv.at[1, :, rows]
+            remote(at, at, kv_send.at[c], kv_recv.at[c], {"sp": here}).wait_recv()
+
+    def await_q(r):
+        at = qx.at[1, pl.ds(r * C, C)]
+        remote(at, at, q_send.at[r], q_recv.at[r], {"sp": here}).wait_recv()
+
+    def far_copy(p):
+        return remote(
+            far.at[pl.ds(p * rows_out, rows_out)],
+            far_r.at[me],
+            af_send.at[p],
+            af_recv.at[me],
+            {"sp": here + 2, "tp": p},
+        )
+
+    def give(r, value):
+        far[pl.ds(r * C, C), :] = value.astype(BF16)
+        for p in range(n_tp):
+            if r * C < (p + 1) * rows_out <= (r + 1) * C:
+                far_copy(p).start()
+
+    @pl.when(here == 0)
+    def _():
+        for r in range(NC):
+            await_q(r)
+            give(r, stick(qx[1, pl.ds(r * C, C), :], 0, NC, False, None)[0])
+
+    @pl.when(here == 1)
+    def _():
+        await_kv()
+        for r in range(NC):
+            await_q(r)
+            q = qx[1, pl.ds(r * C, C), :]
+            nearer, run = stick(q, 0, NC, False, None)
+            give(r, nearer + stick(q, 1, NC, False, run)[0])
+
+    @pl.when(here >= 2)
+    def _():
+        await_kv()
+
+    def exchange(source, landing, send, recv):
+        for d in range(1, n_tp):
+            p = (me + d) % n_tp
+            exchange_copy(source, landing, send, recv, d, p).start()
+        mine = pl.ds(pl.multiple_of(me * rows_out, rows_out), rows_out)
+        landing[me] = source[mine, :]
+
+    def exchange_copy(source, landing, send, recv, d, p):
+        return remote(
+            source.at[pl.ds(pl.multiple_of(p * rows_out, rows_out), rows_out)],
+            landing.at[me],
+            send.at[d],
+            recv.at[me],
+            {"tp": p},
+        )
+
+    def exchanged(source, landing, send, recv):
+        for d in range(1, n_tp):
+            exchange_copy(source, landing, send, recv, d, (me + d) % n_tp).wait_send()
+
+    @pl.when(here >= 1)
+    def _():
+        for r in range(NC):
+            rows = pl.ds(r * C, C)
+            value, run = stick(qx[0, rows, :], 1, NC, False, cons[rows, :])
+            o_acc[rows, :] += value
+            cons[rows, :] = run
+
+    near[...] = o_acc[...].astype(BF16)
+    exchange(near, near_r, an_send, an_recv)
+
+    @pl.when(here >= 2)
+    def _():
+        decay[...] = jnp.exp2(-cons[...]).astype(BF16)
+        exchange(decay, decay_r, ad_send, ad_recv)
+
+    def gather_state(j, incoming):
+        remote(st_buf.at[j], st_buf.at[j], st_send.at[0], st_recv.at[j], {"sp": here}).wait_recv()
+        shrink = st_buf[j, pl.ds(DK, 16), :].astype(F32)
+        kept = shrink[0:1, :] + shrink[8:9, :]
+        return incoming * kept + st_buf[j, pl.ds(0, DK), :].astype(F32)
+
+    incoming = lax.fori_loop(0, here, gather_state, jnp.zeros((DK, DK), F32))
+    combined = local[...] + gdot(qstart[...], incoming.astype(BF16), NT)
+    normed = (
+        combined
+        * lax.rsqrt(jnp.mean(combined * combined, axis=1, keepdims=True) + norm_eps)
+        * hg_s[...]
+    )
+    gate = lin_b[3].astype(F32)
+    lin_o[...] = (normed * (gate / (1.0 + jnp.exp(-gate)))).astype(BF16)
+    exchange(lin_o, lin_r, al_send, al_recv)
+
+    for c in wide:
+        c.wait()
+
+    chips = (chip, x_chip, y_chip, d_chip)
+
+    def arrive(landing, recv, p):
+        remote(landing.at[p], landing.at[p], recv.at[p], recv.at[p], {"tp": p}).wait_recv()
+
+    def product(pair, weight, j, first):
+        at = pl.ds(pl.multiple_of(j * 2 * DK, 2 * DK), 2 * DK)
+        term = fdot(pair, weight[at, :])
+        if first:
+            fin[...] = term
+        else:
+            fin[...] += term
+
+    def pair_of(landing, j):
+        return jnp.concatenate([landing[2 * j], landing[2 * j + 1]], axis=1)
+
+    for j in chips:
+        for p in (2 * j, 2 * j + 1):
+            if j is not chip:
+                arrive(near_r, an_recv, p)
+    arrive(near_r, an_recv, partner)
+
+    @pl.when(here >= 2)
+    def _():
+        for j in chips:
+            for p in (2 * j, 2 * j + 1):
+                if j is not chip:
+                    arrive(decay_r, ad_recv, p)
+        arrive(decay_r, ad_recv, partner)
+        for p in range(n_tp):
+            arrive(far_r, af_recv, p)
+            near_r[p] = (
+                near_r[p].astype(F32) + decay_r[p].astype(F32) * far_r[p].astype(F32)
+            ).astype(BF16)
+
+    for i, j in enumerate(chips):
+        product(pair_of(near_r, j), wos, j, i == 0)
+    for i, j in enumerate(chips):
+        if i:
+            arrive(lin_r, al_recv, 2 * j)
+            arrive(lin_r, al_recv, 2 * j + 1)
+        else:
+            arrive(lin_r, al_recv, partner)
+        if i < len(chips) - 1:
+            product(pair_of(lin_r, j), wol, j, False)
+    at = pl.ds(pl.multiple_of(d_chip * 2 * DK, 2 * DK), 2 * DK)
+    out[...] = (fin[...] + fdot(pair_of(lin_r, d_chip), wol[at, :])).astype(BF16)
+
+    for c in sent:
+        c.wait_send()
+    exchanged(near, near_r, an_send, an_recv)
+    exchanged(lin_o, lin_r, al_send, al_recv)
+
+    @pl.when(here >= 2)
+    def _():
+        exchanged(decay, decay_r, ad_send, ad_recv)
+        for c in range(NC):
+            q_copy(c).wait_send()
+
+    @pl.when(here < 2)
+    def _():
+        for p in range(n_tp):
+            far_copy(p).wait_send()
+
+    for d in range(1, n_sp):
+        later(d, lambda d: st_copy(d).wait_send())
+
+    @pl.when(here + 1 < n_sp)
+    def _():
+        bias_copy().wait_send()
+        for c in range(NC):
+            kv_copy(c).wait_send()
+
+
+def pipelined_call(n_sp, n_tp, args):
+    tokens, lq_w, gd_w, out_linear, out_stick = args[0], args[2], args[9], args[14], args[15]
+    T, F = tokens.shape
+    D, DK = lq_w.shape
+    rank = gd_w.shape[0]
+    rows_out = T // n_tp
+    width = out_linear.shape[1]
+    chunks = T // CHUNK
+    dma = pltpu.SemaphoreType.DMA
+    landing = pltpu.VMEM((n_tp, rows_out, DK), BF16)
+    wide32, wide16 = pltpu.VMEM((T, DK), F32), pltpu.VMEM((T, DK), BF16)
+    return pl.pallas_call(
+        functools.partial(pipelined, n_sp, n_tp),
+        out_shape=pltpu.VMEM((rows_out, width), BF16),
+        in_specs=[pl.BlockSpec(memory_space=pl.ANY)] * len(args),
+        out_specs=pl.BlockSpec(memory_space=pltpu.VMEM),
+        scratch_shapes=[
+            pltpu.VMEM((D,), BF16),
+            pltpu.VMEM((1, DK), F32),
+            pltpu.VMEM((1, T), BF16),
+            pltpu.VMEM((D, 8 * DK), BF16),
+            pltpu.VMEM((rank, D), BF16),
+            pltpu.VMEM((rank, DK), BF16),
+            wide32,
+            pltpu.VMEM(out_linear.shape, BF16),
+            pltpu.VMEM(out_stick.shape, BF16),
+            pltpu.VMEM((n_tp, T, F), BF16),
+            pltpu.VMEM((T, 8 * DK), F32),
+            pltpu.VMEM((T, 128), F32),
+            pltpu.VMEM((4, T, DK), BF16),
+            wide32,
+            wide32,
+            wide16,
+            wide16,
+            pltpu.VMEM((chunks, DK, DK), BF16),
+            pltpu.VMEM((DK, DK), F32),
+            pltpu.VMEM((8, DK), F32),
+            pltpu.VMEM((2, T, DK), BF16),
+            pltpu.VMEM((2, 2, T, DK), BF16),
+            pltpu.VMEM((2, 8, T), F32),
+            pltpu.VMEM((2 * CHUNK, 2 * CHUNK), BF16),
+            wide32,
+            wide32,
+            wide16,
+            wide16,
+            wide16,
+            wide32,
+            pltpu.VMEM((n_sp, DK + 16, DK), BF16),
+            wide16,
+            landing,
+            landing,
+            landing,
+            landing,
+            pltpu.VMEM((rows_out, width), F32),
+            dma((16,)),
+            dma((11 * chunks,)),
+            dma((n_tp, 2 * chunks)),
+            dma((chunks,)),
+            dma((chunks,)),
+            dma((1,)),
+            dma((1,)),
+            dma((chunks,)),
+            dma((chunks,)),
+            dma((n_sp,)),
+            dma((n_sp,)),
+        ]
+        + [dma((n_tp,))] * 8,
+        compiler_params=pltpu.CompilerParams(collective_id=0, has_side_effects=True),
+    )(*args)
+
+
 def per_device(n_sp, n_tp, *args):
     (
         tokens,
@@ -601,6 +1282,26 @@
         out_linear,
         out_stick,
     ) = args
+    operands = (
+        tokens,
+        norm_gain,
+        lin_query,
+        lin_key,
+        lin_value,
+        lin_gate,
+        stick_query,
+        stick_key,
+        stick_value,
+        gate_down.T,
+        gate_up_weight,
+        decay_offset_bias,
+        lin_norm_gain.reshape(1, -1),
+        key_bias,
+        out_linear,
+        out_stick,
+    )
+    if n_sp == 4 and n_tp == 8:
+        return pipelined_call(n_sp, n_tp, operands)
     T, F = tokens.shape
     D, DK = lin_query.shape
     rank = gate_down.shape[1]
@@ -667,24 +1368,7 @@
             dma((n_tp,)),
         ],
         compiler_params=pltpu.CompilerParams(collective_id=0, has_side_effects=True),
-    )(
-        tokens,
-        norm_gain,
-        lin_query,
-        lin_key,
-        lin_value,
-        lin_gate,
-        stick_query,
-        stick_key,
-        stick_value,
-        gate_down.T,
-        gate_up_weight,
-        decay_offset_bias,
-        lin_norm_gain.reshape(1, DK),
-        key_bias,
-        out_linear,
-        out_stick,
-    )
+    )(*operands)
 
 
 def solution(mesh):

time: 33.7 us -> 29.5 us (0.88)
  the two profiles are of different devices: /device:TPU:25 before, /device:TPU:9 now
where the time goes in v2:
time: 29.5 us; the launch traced here: 29.4 us
  Pallas kernels  28.7 us (97%)
  local copies, waits for them, and re-layouts  0.68 us (2%)
    pallas_call x1, Pallas kernels, pipelined_call(): pl.pallas_call(functools.partial(pipelined, n_sp, n_tp), out_shape=pltpu....  28.7 us
    unnamed x1, local copies, waits for them, and re-layouts  0.68 us

profile of v2, /device:TPU:9, one launch (start us, length us, event | category | flops | bytes accessed | tf_op | source)
XLA Modules:
  0.0 29.4 jit_solution(11430472508209301457)
XLA Ops:
  0.0 28.7 %shard_map.154 = bf16[48,2048]{1,0:T(8,128)(2,1)S(1)} custom-call(bf16[384,256]{1,0:T(8,128)(2,1)} %tokens.1, bf16[2048]{0:T(1024)(128)(2,1)} %gain.1, bf16[2048,128]{1,0:T(8,128)(2,1)} %lq_w.1, bf16[2048,128]{1,0:T(8,128)(2,1)} %lk_w.1, bf16[2048,128]{1,0:T(8,128)(2,1)} %lv_w.1, bf16[2048,128]{1,0:T(8,128)(2,1)} %lg_w.1, bf16[2048,128]{1,0:T(8,128)(2,1)} %sq_w.1, ...), custom_call_target="tpu_custom_call" | custom-call | tf_op jit(solution)/shard_map/pallas_call | solution.py:1206
  28.7 0.7 %copy.18 = bf16[48,2048]{1,0:T(8,128)(2,1)} copy(bf16[48,2048]{1,0:T(8,128)(2,1)S(1)} %shard_map.154) | data formatting | bytes 393216
